TPU v7x, 32 devices: a whole 2x2x4 slice. The times are simulated.
32 devices in a mesh: ep: 8 (over z, y), tp: 4 (over x, core).
Axes of the slice: x: 2, y: 2, z: 4, core: 2. Of those that a mesh axis runs over, the one named last changes fastest.
Arguments:
- query: bfloat16 [1024, 1536], P('ep', 'tp'), may hold values from -136 to 136
- latent: bfloat16 [1024, 512], P(('ep', 'tp')), may hold values from -6 to 6
- rope_key: bfloat16 [1024, 32], P(('ep', 'tp')), may hold values from -6 to 6
- latent_gain: float32 [512], replicated, may hold values from 0.1 to 1.9
- key_up: bfloat16 [512, 1024], P(None, 'tp'), may hold values from -0.25 to 0.25
- value_up: bfloat16 [512, 1024], P(None, 'tp'), may hold values from -2 to 2
- out_proj: bfloat16 [1024, 2048], replicated, may hold values from -0.1875 to 0.1875
- tokens: bfloat16 [2048, 2048], P(('ep', 'tp')), may hold values from -6 to 6
- moe_gain: float32 [2048], replicated, may hold values from 0.1 to 1.9
- routes: int32 [2048, 2], P(('ep', 'tp')), may hold values from 0 to 7, all different within a row; in each aligned block of 64 rows (0 to 63, 64 to 127, ...) at most 32 rows name the same one
- group_prob: float32 [2048], P(('ep', 'tp')), may hold values from 0.25 to 1
- expert_prob: float32 [2048, 2], P(('ep', 'tp')), may hold values from 0.02 to 1
- w_gate: bfloat16 [8, 2048, 1024], P('ep', None, 'tp'), may hold values from -0.125 to 0.125
- w_up: bfloat16 [8, 2048, 1024], P('ep', None, 'tp'), may hold values from -0.125 to 0.125
- w_down: bfloat16 [8, 1024, 2048], P('ep', 'tp'), may hold values from -0.1875 to 0.1875
Outputs:
- mixed: bfloat16 [1024, 2048], P(('ep', 'tp'))
- moe_out: bfloat16 [2048, 2048], P(('ep', 'tp'))
Inputs may be any that keep to these rules, and one draw needn't show every extreme that they name: `routes`: each row names 2 different experts; within the rows of one device no expert is named more than 32 times.
All inputs are finite; a program needn't handle non-finite values.
Results may differ from a plain program's by a relative error of at most 0.025.
Values may be sent and summed in bfloat16 or wider, within the bound.
A program may use at most 128 MiB of HBM per device.

v0:
```python
import math

import jax
import jax.numpy as jnp
from jax import lax
from jax.sharding import PartitionSpec as P

NOPE = 64
ROPE_DIM = 32
V_DIM = 64


epsilon = 1e-06
rope_base = 10000.0
masked_value = -1e30


def rms_scale(values, gain):
    widened = values.astype(jnp.float32)
    return widened * lax.rsqrt(jnp.mean(widened * widened, axis=-1, keepdims=True) + epsilon) * gain


def tables(positions, rope_width):
    half_width = rope_width // 2
    inverse = rope_base ** (-2.0 * jnp.arange(half_width, dtype=jnp.float32) / rope_width)
    angles = positions.astype(jnp.float32)[:, None] * inverse[None, :]
    return (jnp.cos(angles), jnp.sin(angles))


def rotate(values, cosine, sine):
    half_width = values.shape[-1] // 2
    lower = values[..., :half_width]
    upper = values[..., half_width:]
    return jnp.concatenate([lower * cosine - upper * sine, lower * sine + upper * cosine], axis=-1)


def keep_state(state_in):
    return state_in


def attend_block(running, query_rot, query_pos, key_part, value_part, rope_part):
    amount = key_part.shape[0]
    span_rows = math.gcd(amount, 1024)
    head_count = query_rot.shape[1]
    scale_factor = query_rot.shape[2] ** (-0.5)
    last_query = query_pos[-1]

    def update(state, block_at):
        row_begin = block_at * span_rows
        keys_here = lax.dynamic_slice_in_dim(key_part, row_begin, span_rows, 0).reshape(
            span_rows, head_count, -1
        )
        values_here = lax.dynamic_slice_in_dim(value_part, row_begin, span_rows, 0).reshape(
            span_rows, head_count, -1
        )
        rope_here = lax.dynamic_slice_in_dim(rope_part, row_begin, span_rows, 0)
        key_pos = row_begin + jnp.arange(span_rows, dtype=jnp.int32)

        def advance(state_in):
            top_old, totals, weighted = state_in
            shared = jnp.broadcast_to(
                rope_here[:, None, :], (span_rows, head_count, rope_here.shape[1])
            )
            full_keys = jnp.concatenate([keys_here, shared], axis=-1)
            scores = (
                jnp.einsum("qhd,khd->hqk", query_rot, full_keys, preferred_element_type=jnp.float32)
                * scale_factor
            )
            allowed = key_pos[None, :] <= query_pos[:, None]
            scores = jnp.where(allowed[None], scores, masked_value)
            top_new = jnp.maximum(top_old, jnp.max(scores, axis=-1))
            raised = jnp.where(allowed[None], jnp.exp(scores - top_new[..., None]), 0.0)
            factor = jnp.exp(top_old - top_new)
            totals = totals * factor + jnp.sum(raised, axis=-1)
            weighted = weighted * factor[..., None] + jnp.einsum(
                "hqk,khd->hqd",
                raised.astype(jnp.bfloat16),
                values_here,
                preferred_element_type=jnp.float32,
            )
            return (top_new, totals, weighted)

        return (lax.cond(key_pos[0] <= last_query, advance, keep_state, state), None)

    running, _ = lax.scan(update, running, jnp.arange(amount // span_rows))
    return running


def mixer_half(query, latent, rope_key, latent_gain, key_up, value_up, out_proj):
    query_rows = query.shape[0]
    own_rows = latent.shape[0]
    query_start = lax.axis_index("ep") * query_rows
    key_start = query_start + lax.axis_index("tp") * own_rows
    head_count = query.shape[1] // (NOPE + ROPE_DIM)
    normed = rms_scale(latent, latent_gain).astype(jnp.bfloat16)
    key_cos, key_sin = tables(key_start + jnp.arange(own_rows, dtype=jnp.int32), ROPE_DIM)
    rotated_key = rotate(rope_key.astype(jnp.float32), key_cos, key_sin).astype(jnp.bfloat16)
    query_pos = query_start + jnp.arange(query_rows, dtype=jnp.int32)
    query_cos, query_sin = tables(query_pos, ROPE_DIM)
    query_heads = query.reshape(query_rows, head_count, NOPE + ROPE_DIM)
    turned = rotate(
        query_heads[..., NOPE:].astype(jnp.float32), query_cos[:, None, :], query_sin[:, None, :]
    ).astype(jnp.bfloat16)
    query_rot = jnp.concatenate([query_heads[..., :NOPE], turned], axis=-1)
    last_query = query_start + query_rows - 1
    initial = (
        jnp.full((head_count, query_rows), masked_value, jnp.float32),
        jnp.zeros((head_count, query_rows), jnp.float32),
        jnp.zeros((head_count, query_rows, V_DIM), jnp.float32),
    )
    shard_rows = (
        lax.all_gather(normed, ("ep", "tp"), axis=0, tiled=True),
        lax.all_gather(rotated_key, ("ep", "tp"), axis=0, tiled=True),
    )

    def compute(state_in):
        key_part = jnp.dot(shard_rows[0], key_up, preferred_element_type=jnp.float32).astype(
            jnp.bfloat16
        )
        value_part = jnp.dot(shard_rows[0], value_up, preferred_element_type=jnp.float32).astype(
            jnp.bfloat16
        )
        return attend_block(state_in, query_rot, query_pos, key_part, value_part, shard_rows[1])

    running = lax.cond(jnp.int32(0) <= last_query, compute, keep_state, initial)
    totals = running[1]
    weighted = running[2]
    attention = (
        (weighted / totals[..., None])
        .transpose(1, 0, 2)
        .reshape(query_rows, head_count * V_DIM)
        .astype(jnp.bfloat16)
    )
    own_attention = lax.all_to_all(attention, "tp", split_axis=0, concat_axis=1, tiled=True)
    return jnp.dot(own_attention, out_proj, preferred_element_type=jnp.float32).astype(jnp.bfloat16)


def expert_half(tokens, moe_gain, routes, group_prob, expert_prob, w_gate, w_up, w_down):
    row_count, model_width = tokens.shape
    top_count = routes.shape[1]
    expert_count = lax.axis_size("ep")
    capacity = 2 * top_count * row_count // expert_count
    normed = rms_scale(tokens, moe_gain).astype(jnp.bfloat16)
    flat_routes = routes.reshape(-1)
    onehot = (flat_routes[:, None] == jnp.arange(expert_count, dtype=jnp.int32)[None, :]).astype(
        jnp.int32
    )
    earlier = jnp.cumsum(onehot, axis=0) - onehot
    slot_index = jnp.sum(earlier * onehot, axis=1)
    target = flat_routes * capacity + slot_index
    owner = target[None, :] == jnp.arange(expert_count * capacity, dtype=jnp.int32)[:, None]
    dispatch_table = jnp.any(
        owner.reshape(expert_count * capacity, row_count, top_count), axis=2
    ).astype(jnp.bfloat16)
    outgoing = jnp.dot(dispatch_table, normed, preferred_element_type=jnp.float32).astype(
        jnp.bfloat16
    )
    outgoing = outgoing.reshape(expert_count, capacity, model_width)
    arrived = lax.all_to_all(outgoing, "ep", split_axis=0, concat_axis=0, tiled=True)
    sources, slots, _ = arrived.shape
    flat_rows = arrived.reshape(sources * slots, model_width)
    shard_rows = lax.all_gather(flat_rows, "tp", axis=0, tiled=True)
    gate_values = jnp.dot(shard_rows, w_gate[0], preferred_element_type=jnp.float32)
    up_values = jnp.dot(shard_rows, w_up[0], preferred_element_type=jnp.float32)
    hidden = (jax.nn.silu(gate_values) * up_values).astype(jnp.bfloat16)

    def lower(offset, amount):
        return jnp.dot(hidden, w_down[0], preferred_element_type=jnp.float32)

    summed = lax.psum_scatter(
        lower(jnp.int32(0), sources * slots * lax.axis_size("tp")).astype(jnp.bfloat16),
        "tp",
        scatter_dimension=0,
        tiled=True,
    )
    result = summed.reshape(sources, slots, model_width)
    returned = lax.all_to_all(result, "ep", split_axis=0, concat_axis=0, tiled=True)
    returned_flat = returned.reshape(expert_count * capacity, model_width)
    picked = returned_flat[target].reshape(row_count, top_count, model_width).astype(jnp.float32)
    shares = group_prob[:, None] * expert_prob / jnp.sum(expert_prob, axis=1, keepdims=True)
    return jnp.sum(shares[:, :, None] * picked, axis=1).astype(jnp.bfloat16)


def body(
    query,
    latent,
    rope_key,
    latent_gain,
    key_up,
    value_up,
    out_proj,
    tokens,
    moe_gain,
    routes,
    group_prob,
    expert_prob,
    w_gate,
    w_up,
    w_down,
):
    mixed = mixer_half(query, latent, rope_key, latent_gain, key_up, value_up, out_proj)
    moe_out = expert_half(tokens, moe_gain, routes, group_prob, expert_prob, w_gate, w_up, w_down)
    return (mixed, moe_out)


def solution(mesh):
    return jax.shard_map(
        body,
        mesh=mesh,
        in_specs=(
            P("ep", "tp"),
            P(("ep", "tp"), None),
            P(("ep", "tp"), None),
            P(),
            P(None, "tp"),
            P(None, "tp"),
            P(),
            P(("ep", "tp"), None),
            P(),
            P(("ep", "tp"), None),
            P(("ep", "tp")),
            P(("ep", "tp"), None),
            P("ep", None, "tp"),
            P("ep", None, "tp"),
            P("ep", "tp", None),
        ),
        out_specs=(P(("ep", "tp"), None), P(("ep", "tp"), None)),
        check_vma=False,
    )
```

profile of v0, /device:TPU:0, one launch (start us, length us, event | category | flops | bytes accessed | tf_op | source)
XLA Modules:
  0.0 223.9 jit_solution(14774280976944361633)
XLA Ops:
  9.6 1.1 fusion.27
  10.8 1.6 convolution_convert_fusion.3
  12.3 33.0 %all_to_all.26 = bf16[8,32,2048]{2,1,0:T(8,128)(2,1)} all-to-all(bf16[8,32,2048]{2,1,0:T(8,128)(2,1)S(1)} %bitcast.53), channel_id=1, replica_groups=mesh['ep'=8,'tp'=4] {'ep'}, dimensions={0} | all-to-all | bytes 2097152 | tf_op jit(solution)/shard_map/all_to_all | solution.py:159
  46.3 32.6 %all-gather.5.cloned.1.call-done = bf16[1024,2048]{1,0:T(8,128)(2,1)} async-done(((bf16[256,2048]{1,0:T(8,128)(2,1)}), bf16[1024,2048]{1,0:T(8,128)(2,1)}) %all-gather.5.cloned.1.call-update) | async-done | bytes 4194320 | tf_op jit(solution)/shard_map/all_gather | solution.py:162
  78.9 4.4 %fusion.20 = f32[1024,256]{1,0:T(8,128)} fusion(bf16[1024,2048]{1,0:T(8,128)(2,1)} %all-gather.5.cloned.1.call-done, bf16[1,2048,256]{2,1,0:T(8,128)(2,1)S(1)} %copy-done.11), kind=kOutput, calls=%fused_computation.33 | convolution fusion | flops 1073741824 | bytes 6291456 | tf_op jit(solution)/shard_map/dot_general | solution.py:163
  83.3 8.8 %convolution_convert_fusion.2 = bf16[1024,2048]{1,0:T(8,128)(2,1)} fusion(bf16[1024,2048]{1,0:T(8,128)(2,1)} %all-gather.5.cloned.1.call-done, bf16[1,256,2048]{2,1,0:T(8,128)(2,1)S(1)} %copy-done, bf16[1,2048,256]{2,1,0:T(8,128)(2,1)S(1)} %copy-done.12, f32[1024,256]{1,0:T(8,128)} %fusion.20), kind=kOutput, calls=%fused_computation.26 | convolution fusion | flops 2151153664 | bytes 11534336 | tf_op jit(solution)/shard_map/dot_general | solution.py:168
  92.2 0.8 copy-done.6
  93.5 41.5 %all_gather.10 = bf16[1024,32]{1,0:T(8,128)(2,1)S(1)} all-gather(bf16[32,32]{1,0:T(8,128)(2,1)S(1)} %copy.62), channel_id=1, replica_groups=mesh['ep'=8,'tp'=4] {'ep','tp'}, dimensions={0}, use_global_device_ids=true | all-gather | bytes 67584 | tf_op jit(solution)/shard_map/all_gather | solution.py:113
  135.2 1.1 all-gather.3.cloned.1.call-done
  136.2 14.5 %conditional.2 = ((f32[4,128]{1,0:T(4,128)}, f32[4,128,64]{1,2,0:T(8,128)})) conditional(s32[]{:T(128)} %convert_element_type.90, () %tuple.32, (s32[]{:T(128)}, s32[128]{0:T(128)S(1)}, bf16[1024,512]{1,0:T(8,128)(2,1)}, bf16[512,256]{1,0:T(8,128)(2,1)S(1)}, bf16[512,256]{1,0:T(8,128)(2,1)S(1)}, /*index=5*/bf16[1024,32]{1,0:T(8,128)(2,1)S(1)}, ...), branch_computations={%region_1.0_spmd, %region_2.7_spmd} | conditional | flops 713754240 | bytes 23273134 | solution.py:125
  136.2 1.7 convolution_convert_fusion
  137.9 1.7 convolution_convert_fusion.1
  143.2 7.5 %conditional = ((f32[4,128]{1,0:T(4,128)}, f32[4,128,64]{1,2,0:T(8,128)})) conditional(s32[]{:T(128)} %bitcast.3, (f32[4,128]{1,0:T(4,128)}, f32[4,128,64]{1,2,0:T(8,128)}) %tuple.26, (s32[1024]{0:T(1024)S(1)}, s32[128]{0:T(128)S(1)}, bf16[1024,256]{1,0:T(8,128)(2,1)S(1)}, bf16[1024,32]{1,0:T(8,128)(2,1)S(1)}, bf16[128,4,96]{0,2,1:T(8,128)(2,1)S(1)}, ...), branch_computations={%region_3.3_spmd, %region_4.6_spmd} | conditional | flops 176358912 | bytes 19460660 | solution.py:83
  144.4 1.3 copy-done.1
  146.3 1.2 subtract_exponential_fusion
  147.7 3.1 %convolution_add_fusion = f32[4,128,64]{1,2,0:T(8,128)} fusion(bf16[1024,4,64]{0,2,1:T(8,128)(2,1)S(1)} %bitcast.56, f32[4,1024,128]{2,1,0:T(8,128)} %copy-done.1, f32[4,128]{1,0:T(4,128)S(1)} %broadcast_maximum_fusion, pred[128,1024]{0,1:T(8,128)(4,1)S(1)} %broadcast_compare_fusion, f32[4,128,64]{1,2,0:T(8,128)} %get-tuple-element.110, ...), kind=kOutput, calls=%fused_computation.6 | convolution fusion | flops 69795840 | bytes 3018752 | tf_op jit(solution)/shard_map/cond/branch_1_fun/while/body/eval_jaxpr/cond/branch_1_fun/hqk,khd->hqd/dot_general | solution.py:75
  150.7 1.0 fusion.39
  152.0 6.6 %all_to_all.27 = bf16[4,32,256]{2,1,0:T(8,128)(2,1)S(1)} all-to-all(bf16[4,32,256]{2,1,0:T(8,128)(2,1)S(1)} %convert_element_type.99), channel_id=1, replica_groups=mesh['ep'=8,'tp'=4] {'tp'}, dimensions={0} | all-to-all | bytes 131072 | tf_op jit(solution)/shard_map/all_to_all | solution.py:134
  158.6 23.9 %reduce-scatter.2.cloned.1.call-done = bf16[256,2048]{1,0:T(8,128)(2,1)} async-done(((bf16[1024,2048]{1,0:T(8,128)(2,1)}), bf16[256,2048]{1,0:T(8,128)(2,1)}) %reduce-scatter.2.cloned.1.call-update) | async-done | bytes 1048592 | tf_op jit(solution)/shard_map/reduce_scatter | solution.py:170
  182.5 5.4 %all-to-all-start.2 = ((bf16[8,32,2048]{2,1,0:T(8,128)(2,1)}), bf16[8,32,2048]{2,1,0:T(8,128)(2,1)S(1)}, u32[]{:S(2)}, u32[]{:S(2)}) async-start(bf16[8,32,2048]{2,1,0:T(8,128)(2,1)} %bitcast.54), calls=%async_computation.3 | async-start | bytes 2097152 | tf_op jit(solution)/shard_map/all_to_all | solution.py:177
  188.2 3.7 %convolution_convert_fusion.4 = bf16[32,2048]{1,0:T(8,128)(2,1)} fusion(bf16[32,1024]{1,0:T(8,128)(2,1)S(1)} %bitcast.59, bf16[1024,2048]{1,0:T(8,128)(2,1)} %param.25), kind=kOutput, calls=%fused_computation.28 | convolution fusion | flops 134283264 | bytes 4390912 | tf_op jit(solution)/shard_map/dot_general | solution.py:135
  191.9 21.7 %all-to-all-done.2 = bf16[8,32,2048]{2,1,0:T(8,128)(2,1)S(1)} async-done(((bf16[8,32,2048]{2,1,0:T(8,128)(2,1)}), bf16[8,32,2048]{2,1,0:T(8,128)(2,1)S(1)}, u32[]{:S(2)}, u32[]{:S(2)}) %all-to-all-start.2) | async-done | bytes 1048608 | tf_op jit(solution)/shard_map/all_to_all | solution.py:177
  213.6 0.9 gather_fusion
  215.2 2.2 multiply_reduce_fusion
  (83 shorter events, 9.5 us)
Async XLA Ops:
  7.2 76.2 %copy-start = (bf16[1,256,2048]{2,1,0:T(8,128)(2,1)S(1)}, bf16[1,256,2048]{2,1,0:T(8,128)(2,1)}, u32[]{:S(2)}) copy-start(bf16[1,256,2048]{2,1,0:T(8,128)(2,1)} %param.33) | copy-start | bytes 3145732
  7.2 71.8 %all-gather.5.cloned.1.call-start = ((), (), s32[]{:S(2)}) async-start(), calls=%async_computation.5 | async-start | bytes 5242880 | tf_op jit(solution)/shard_map/all_gather | solution.py:162
  10.7 34.6 %copy-start.4 = (bf16[32,512]{1,0:T(8,128)(2,1)S(1)}, bf16[32,512]{1,0:T(8,128)(2,1)}, u32[]{:S(2)}) copy-start(bf16[32,512]{1,0:T(8,128)(2,1)} %param.20) | copy-start | bytes 98308
  10.7 34.8 %copy-start.9 = (f32[512]{0:T(512)S(1)}, f32[512]{0:T(512)}, u32[]{:S(2)}) copy-start(f32[512]{0:T(512)} %param.22) | copy-start | bytes 6148
  10.8 68.2 %copy-start.11 = (bf16[1,2048,256]{2,1,0:T(8,128)(2,1)S(1)}, bf16[1,2048,256]{2,1,0:T(8,128)(2,1)}, u32[]{:S(2)}) copy-start(bf16[1,2048,256]{2,1,0:T(8,128)(2,1)} %param.31) | copy-start | bytes 3145732
  45.3 90.9 %all-gather.3.cloned.1.call-start = ((), (), s32[]{:S(2)}) async-start(), calls=%async_computation.4 | async-start | bytes 1081344 | tf_op jit(solution)/shard_map/all_gather | solution.py:112
  46.2 37.1 %copy-start.12 = (bf16[1,2048,256]{2,1,0:T(8,128)(2,1)S(1)}, bf16[1,2048,256]{2,1,0:T(8,128)(2,1)}, u32[]{:S(2)}) copy-start(bf16[1,2048,256]{2,1,0:T(8,128)(2,1)} %param.32) | copy-start | bytes 3145732
  46.2 136.3 %reduce-scatter.2.cloned.1.call-start = ((), (), s32[]{:S(2)}) async-start(), calls=%async_computation.6 | async-start | bytes 5242880 | tf_op jit(solution)/shard_map/reduce_scatter | solution.py:170
  92.1 0.9 copy-start.6
  92.1 1.0 copy-start.7
  92.1 44.1 %copy-start.2 = (bf16[512,256]{1,0:T(8,128)(2,1)S(1)}, bf16[512,256]{1,0:T(8,128)(2,1)}, u32[]{:S(2)}) copy-start(bf16[512,256]{1,0:T(8,128)(2,1)} %param.23) | copy-start | bytes 786436
  92.1 44.1 %copy-start.3 = (bf16[512,256]{1,0:T(8,128)(2,1)S(1)}, bf16[512,256]{1,0:T(8,128)(2,1)}, u32[]{:S(2)}) copy-start(bf16[512,256]{1,0:T(8,128)(2,1)} %param.24) | copy-start | bytes 786436
  144.4 1.3 copy-start.1
  150.7 37.2 %copy-start.5 = (s32[64,2]{1,0:T(8,128)S(1)}, s32[64,2]{1,0:T(8,128)}, u32[]{:S(2)}) copy-start(s32[64,2]{1,0:T(8,128)} %get-tuple-element.197) | copy-start | bytes 1540
  150.7 37.3 %copy-start.8 = (f32[64,2]{0,1:T(2,128)S(1)}, f32[64,2]{0,1:T(2,128)}, u32[]{:S(2)}) copy-start(f32[64,2]{0,1:T(2,128)} %param.30) | copy-start | bytes 1540
  150.7 37.4 %copy-start.10 = (f32[64]{0:T(128)S(1)}, f32[64]{0:T(128)}, u32[]{:S(2)}) copy-start(f32[64]{0:T(128)} %param.29) | copy-start | bytes 772
  182.5 31.1 %all-to-all-start.2 = ((bf16[8,32,2048]{2,1,0:T(8,128)(2,1)}), bf16[8,32,2048]{2,1,0:T(8,128)(2,1)S(1)}, u32[]{:S(2)}, u32[]{:S(2)}) async-start(bf16[8,32,2048]{2,1,0:T(8,128)(2,1)} %bitcast.54), calls=%async_computation.3 | async-start | bytes 2097152 | tf_op jit(solution)/shard_map/all_to_all | solution.py:177
Sparse Core Ops, SparseCore 0:
  45.4 33.4 all-gather.4
  82.4 53.8 all-gather.2
  138.8 43.6 reduce-scatter.1
where the time goes:
time: 225 us; the launch traced here: 224 us
  blocking collectives  81.1 us (36%)
  waiting for transfers between devices  79.3 us (35%)
  matrix products  25.4 us (11%)
  between operations  14 us (6%)
  local copies, waits for them, and re-layouts  8.74 us (4%)
  other arithmetic  8.56 us (4%)
  starting transfers between devices  5.53 us (2%)
    all_gather x1, blocking collectives, mixer_half(): lax.all_gather(rotated_key, ('ep', 'tp'), axis=0, tiled=True)  41.5 us
    all_to_all x1, blocking collectives, expert_half(): lax.all_to_all(outgoing, 'ep', split_axis=0, concat_axis=0, tiled=True)  33 us
    all_gather x1, waiting for transfers between devices, expert_half(): shard_rows = lax.all_gather(flat_rows, 'tp', axis=0, tiled=True)  32.6 us
    reduce_scatter x1, waiting for transfers between devices, expert_half(): lax.psum_scatter(lower(jnp.int32(0), sources * slots * lax.axis_size('tp'...  23.9 us
    all_to_all x1, waiting for transfers between devices, expert_half(): lax.all_to_all(result, 'ep', split_axis=0, concat_axis=0, tiled=True)  21.7 us
    dot_general x1, matrix products, lower(): return jnp.dot(hidden, w_down[0], preferred_element_type=jnp.float32)  8.77 us
    all_to_all x1, blocking collectives, mixer_half(): lax.all_to_all(attention, 'tp', split_axis=0, concat_axis=1, tiled=True)  6.64 us
    all_to_all x1, starting transfers between devices, expert_half(): lax.all_to_all(result, 'ep', split_axis=0, concat_axis=0, tiled=True)  5.41 us
  transfers between devices with their start and end apart: 4, of which 4 were waited for; matrix products, arithmetic and copies ran while one was open for 14% of the time, Pallas kernels for 0%

commit v1 on v0

--- a/solution.py
+++ b/solution.py
@@ -1,8 +1,11 @@
+import functools
 import math
 
 import jax
 import jax.numpy as jnp
 from jax import lax
+from jax.experimental import pallas as pl
+from jax.experimental.pallas import tpu as pltpu
 from jax.sharding import PartitionSpec as P
 
 NOPE = 64
@@ -203,9 +206,450 @@
     return (mixed, moe_out)
 
 
-def solution(mesh):
+def both_halves(
+    heads,
+    rope_width,
+    outgoing,
+    lat_own,
+    query_big,
+    key_up,
+    value_up,
+    out_proj_hbm,
+    gate_hbm,
+    up_hbm,
+    down_hbm,
+    mixed,
+    returned,
+    arrived,
+    lat_all,
+    partial,
+    from_pair,
+    pair_sum,
+    from_far,
+    result,
+    keys,
+    heads_own,
+    heads_all,
+    out_proj,
+    gate,
+    up,
+    down,
+    load_sem,
+    send_sem,
+    recv_sem,
+    head_send,
+    head_recv,
+):
+    experts, capacity, width = outgoing.shape
+    n_tp = lat_all.shape[1]
+    me = lax.axis_index("ep")
+    tp = lax.axis_index("tp")
+    mate = tp + 1 - 2 * (tp % 2)
+    far = (tp + 2) % n_tp
+    cross = (mate + 2) % n_tp
+
+    loads = [
+        pltpu.make_async_copy(gate_hbm, gate, load_sem.at[0]),
+        pltpu.make_async_copy(up_hbm, up, load_sem.at[1]),
+        pltpu.make_async_copy(down_hbm, down, load_sem.at[2]),
+        pltpu.make_async_copy(out_proj_hbm, out_proj, load_sem.at[3]),
+        pltpu.make_async_copy(outgoing.at[me], arrived.at[me, tp], load_sem.at[4]),
+        pltpu.make_async_copy(lat_own, lat_all.at[me, tp], load_sem.at[5]),
+    ]
+    for load in loads:
+        load.start()
+
+    def remote(src, dst, kind, step, device):
+        return pltpu.make_async_remote_copy(
+            src_ref=src,
+            dst_ref=dst,
+            send_sem=send_sem.at[kind, step],
+            recv_sem=recv_sem.at[kind, step],
+            device_id=device,
+            device_id_type=pl.DeviceIdType.MESH,
+        )
+
+    barrier = pltpu.get_barrier_semaphore()
+
+    def greet(step, carry):
+        pl.semaphore_signal(
+            barrier,
+            inc=1,
+            device_id={"ep": (me + step) % experts},
+            device_id_type=pl.DeviceIdType.MESH,
+        )
+        return carry
+
+    lax.fori_loop(1, experts, greet, 0)
+    for peer in (mate, far, cross):
+        pl.semaphore_signal(
+            barrier, inc=1, device_id={"tp": peer}, device_id_type=pl.DeviceIdType.MESH
+        )
+    pl.semaphore_wait(barrier, experts + 2)
+
+    def ep_rows(step, slot):
+        target = (me + step) % experts
+        return remote(outgoing.at[target], arrived.at[slot, tp], 0, step, {"ep": target})
+
+    def ep_lat(step, slot):
+        target = (me + step) % experts
+        return remote(lat_own, lat_all.at[slot, tp], 1, step, {"ep": target})
+
+    def hop_rows(kind, step, block, peer):
+        source = (me + experts - step) % experts
+        place = arrived.at[source, block]
+        return remote(place, place, kind, step, {"tp": peer})
+
+    def hop_lat(kind, step, block, peer):
+        source = (me + experts - step) % experts
+        place = lat_all.at[source, block]
+        return remote(place, place, kind, step, {"tp": peer})
+
+    def to_mate(kind, step, block, part):
+        source = (me + experts - step) % experts
+        return remote(
+            partial.at[source, block], from_pair.at[source, part], kind, step, {"tp": mate}
+        )
+
+    def to_far(step):
+        source = (me + experts - step) % experts
+        return remote(pair_sum.at[source], from_far.at[source], 10, step, {"tp": far})
+
+    def back(step, slot):
+        source = (me + experts - step) % experts
+        return remote(result.at[source], returned.at[slot], 11, step, {"ep": source})
+
+    def send_all(step, carry):
+        ep_lat(step, me).start()
+        return carry
+
+    lax.fori_loop(1, experts, send_all, 0)
+
+    def send_rows(step, carry):
+        ep_rows(step, me).start()
+        return carry
+
+    lax.fori_loop(1, experts, send_rows, 0)
+    for load in loads[4:]:
+        load.wait()
+
+    def forward(step):
+        source = (me + experts - step) % experts
+
+        @pl.when(step > 0)
+        def _():
+            ep_lat(step, source).wait_recv()
+            ep_rows(step, source).wait_recv()
+
+        hop_lat(5, step, tp, far).start()
+        hop_rows(4, step, tp, far).start()
+        hop_lat(3, step, tp, mate).start()
+        hop_rows(2, step, tp, mate).start()
+
+    def relay(step):
+        hop_lat(5, step, far, far).wait_recv()
+        hop_rows(4, step, far, far).wait_recv()
+        hop_lat(7, step, far, mate).start()
+        hop_rows(6, step, far, mate).start()
+
+    def compute(step):
+        source = (me + experts - step) % experts
+        hop_lat(3, step, mate, mate).wait_recv()
+        hop_rows(2, step, mate, mate).wait_recv()
+        hop_lat(7, step, cross, mate).wait_recv()
+        hop_rows(6, step, cross, mate).wait_recv()
+
+        @pl.when(step == 0)
+        def _():
+            for load in loads[:3]:
+                load.wait()
+
+        rows = arrived[source].reshape(n_tp * capacity, width)
+        gate_values = jnp.dot(rows, gate[...], preferred_element_type=jnp.float32)
+        up_values = jnp.dot(rows, up[...], preferred_element_type=jnp.float32)
+        hidden = (gate_values / (1.0 + jnp.exp(-gate_values)) * up_values).astype(jnp.bfloat16)
+        product = jnp.dot(hidden, down[...], preferred_element_type=jnp.float32)
+        partial[source] = product.astype(jnp.bfloat16).reshape(n_tp, capacity, width)
+        to_mate(9, step, cross, 1).start()
+        to_mate(8, step, mate, 0).start()
+
+    def reduce_pair(step):
+        source = (me + experts - step) % experts
+        to_mate(9, step, cross, 1).wait_recv()
+        pair_sum[source] = (
+            partial[source, far].astype(jnp.float32) + from_pair[source, 1].astype(jnp.float32)
+        ).astype(jnp.bfloat16)
+        to_far(step).start()
+
+    def reduce_far(step):
+        source = (me + experts - step) % experts
+        to_mate(8, step, mate, 0).wait_recv()
+        to_far(step).wait_recv()
+        result[source] = (
+            partial[source, tp].astype(jnp.float32)
+            + from_pair[source, 0].astype(jnp.float32)
+            + from_far[source].astype(jnp.float32)
+        ).astype(jnp.bfloat16)
+
+        @pl.when(step > 0)
+        def _():
+            back(step, me).start()
+
+        @pl.when(step == 0)
+        def _():
+            returned[me] = result[me]
+
+    def attend():
+        rows = query_big.shape[1]
+        latent_width = key_up.shape[0]
+        nope_width = key_up.shape[1]
+        value_width = value_up.shape[1] // heads
+        packed = lat_all[...].reshape(-1, lat_all.shape[-1])
+        normed = packed[:, :latent_width]
+        seq = packed.shape[0]
+        keys[:, :nope_width] = jnp.dot(
+            normed, key_up[...], preferred_element_type=jnp.float32
+        ).astype(jnp.bfloat16)
+        keys[:, nope_width:] = packed[:, latent_width:]
+        values = jnp.dot(normed, value_up[...], preferred_element_type=jnp.float32).astype(
+            jnp.bfloat16
+        )
+        query_pos = me * rows + lax.broadcasted_iota(jnp.int32, (rows, seq), 0)
+        allowed = lax.broadcasted_iota(jnp.int32, (rows, seq), 1) <= query_pos
+        lane = lax.broadcasted_iota(jnp.int32, (rows, heads * value_width), 1)
+        scale = (nope_width // heads + rope_width) ** (-0.5)
+        gathered = jnp.zeros((rows, heads * value_width), jnp.float32)
+        for head in range(heads):
+            scores = (
+                lax.dot_general(
+                    query_big[head],
+                    keys[...],
+                    (((1,), (1,)), ((), ())),
+                    preferred_element_type=jnp.float32,
+                )
+                * scale
+            )
+            scores = jnp.where(allowed, scores, masked_value)
+            raised = jnp.exp(scores - jnp.max(scores, axis=1, keepdims=True))
+            totals = jnp.sum(raised, axis=1, keepdims=True)
+            weighted = jnp.dot(
+                raised.astype(jnp.bfloat16), values, preferred_element_type=jnp.float32
+            )
+            inside = (lane >= head * value_width) & (lane < (head + 1) * value_width)
+            gathered = jnp.where(inside, weighted / totals, gathered)
+        heads_own[...] = gathered.astype(jnp.bfloat16).reshape(heads_own.shape)
+
+    def head_copy(number, peer, slot):
+        return pltpu.make_async_remote_copy(
+            src_ref=heads_own.at[peer],
+            dst_ref=heads_all.at[slot],
+            send_sem=head_send.at[number],
+            recv_sem=head_recv.at[number],
+            device_id={"tp": peer},
+            device_id_type=pl.DeviceIdType.MESH,
+        )
+
+    def stage(turn, carry):
+        @pl.when(turn < experts)
+        def _():
+            forward(turn)
+
+        @pl.when((turn >= 1) & (turn < experts + 1))
+        def _():
+            relay(turn - 1)
+
+        @pl.when((turn >= 2) & (turn < experts + 2))
+        def _():
+            compute(turn - 2)
+
+        @pl.when((turn >= 3) & (turn < experts + 3))
+        def _():
+            reduce_pair(turn - 3)
+
+        @pl.when(turn >= 4)
+        def _():
+            reduce_far(turn - 4)
+
+        return carry
+
+    lax.fori_loop(0, experts + 4, stage, 0)
+
+    attend()
+    peers = (mate, far, cross)
+    for number, peer in enumerate(peers):
+        head_copy(number, peer, tp).start()
+    heads_all[tp] = heads_own[tp]
+    loads[3].wait()
+    for number, peer in enumerate(peers):
+        head_copy(number, peer, peer).wait_recv()
+    depth = heads_all.shape[2]
+    total = jnp.zeros(mixed.shape, jnp.float32)
+    for part in range(n_tp):
+        total = total + jnp.dot(
+            heads_all[part],
+            out_proj[part * depth : (part + 1) * depth, :],
+            preferred_element_type=jnp.float32,
+        )
+    mixed[...] = total.astype(mixed.dtype)
+
+    def finish(step, carry):
+        ep_lat(step, me).wait_send()
+        ep_rows(step, me).wait_send()
+        back(step, me).wait_send()
+        back(step, (me + step) % experts).wait_recv()
+        return carry
+
+    lax.fori_loop(1, experts, finish, 0)
+
+    def finish_tp(step, carry):
+        hop_lat(5, step, tp, far).wait_send()
+        hop_rows(4, step, tp, far).wait_send()
+        hop_lat(3, step, tp, mate).wait_send()
+        hop_rows(2, step, tp, mate).wait_send()
+        hop_lat(7, step, far, mate).wait_send()
+        hop_rows(6, step, far, mate).wait_send()
+        to_mate(9, step, cross, 1).wait_send()
+        to_mate(8, step, mate, 0).wait_send()
+        to_far(step).wait_send()
+        return carry
+
+    lax.fori_loop(0, experts, finish_tp, 0)
+    for number, peer in enumerate(peers):
+        head_copy(number, peer, tp).wait_send()
+
+
+def padded(amount):
+    return -(-amount // 128) * 128
+
+
+def fused_body(
+    query,
+    latent,
+    rope_key,
+    latent_gain,
+    key_up,
+    value_up,
+    out_proj,
+    tokens,
+    moe_gain,
+    routes,
+    group_prob,
+    expert_prob,
+    w_gate,
+    w_up,
+    w_down,
+):
+    n_ep = lax.axis_size("ep")
+    n_tp = lax.axis_size("tp")
+    query_rows = query.shape[0]
+    own_rows, latent_width = latent.shape
+    query_start = lax.axis_index("ep") * query_rows
+    key_start = query_start + lax.axis_index("tp") * own_rows
+    heads = query.shape[1] // (NOPE + ROPE_DIM)
+    normed_latent = rms_scale(latent, latent_gain).astype(jnp.bfloat16)
+    key_cos, key_sin = tables(key_start + jnp.arange(own_rows, dtype=jnp.int32), ROPE_DIM)
+    rotated_key = rotate(rope_key.astype(jnp.float32), key_cos, key_sin).astype(jnp.bfloat16)
+    rope_room = padded(ROPE_DIM)
+    gap = rope_room - ROPE_DIM
+    lat_own = jnp.concatenate([normed_latent, jnp.pad(rotated_key, ((0, 0), (0, gap)))], axis=1)
+    query_cos, query_sin = tables(query_start + jnp.arange(query_rows, dtype=jnp.int32), ROPE_DIM)
+    query_heads = query.reshape(query_rows, heads, NOPE + ROPE_DIM).transpose(1, 0, 2)
+    turned = rotate(
+        query_heads[..., NOPE:].astype(jnp.float32), query_cos[None], query_sin[None]
+    ).astype(jnp.bfloat16)
+    own_head = jnp.eye(heads, dtype=jnp.bool_)[:, None, :, None]
+    spread = jnp.where(own_head, query_heads[:, :, None, :NOPE], jnp.bfloat16(0)).reshape(
+        heads, query_rows, heads * NOPE
+    )
+    query_big = jnp.concatenate(
+        [spread, jnp.pad(turned, ((0, 0), (0, 0), (0, gap)))], axis=-1
+    )
+
+    row_count, width = tokens.shape
+    top_count = routes.shape[1]
+    capacity = 2 * top_count * row_count // n_ep
+    normed = rms_scale(tokens, moe_gain).astype(jnp.bfloat16)
+    flat_routes = routes.reshape(-1)
+    onehot = (flat_routes[:, None] == jnp.arange(n_ep, dtype=jnp.int32)[None, :]).astype(jnp.int32)
+    earlier = jnp.cumsum(onehot, axis=0) - onehot
+    slot_index = jnp.sum(earlier * onehot, axis=1)
+    target = flat_routes * capacity + slot_index
+    owner = target[None, :] == jnp.arange(n_ep * capacity, dtype=jnp.int32)[:, None]
+    dispatch_table = jnp.any(owner.reshape(n_ep * capacity, row_count, top_count), axis=2).astype(
+        jnp.bfloat16
+    )
+    outgoing = jnp.dot(dispatch_table, normed, preferred_element_type=jnp.float32).astype(
+        jnp.bfloat16
+    )
+    outgoing = outgoing.reshape(n_ep, capacity, width)
+
+    bf16 = jnp.bfloat16
+    lat_width = latent_width + rope_room
+    vmem = pl.BlockSpec(memory_space=pltpu.VMEM)
+    anywhere = pl.BlockSpec(memory_space=pl.ANY)
+    mixed, returned = pl.pallas_call(
+        functools.partial(both_halves, heads, ROPE_DIM),
+        out_shape=(
+            jax.ShapeDtypeStruct((own_rows, out_proj.shape[1]), bf16),
+            jax.ShapeDtypeStruct((n_ep, capacity, width), bf16),
+        ),
+        in_specs=[vmem] * 5 + [anywhere] * 4,
+        out_specs=(vmem, vmem),
+        scratch_shapes=[
+            pltpu.VMEM((n_ep, n_tp, capacity, width), bf16),
+            pltpu.VMEM((n_ep, n_tp, own_rows, lat_width), bf16),
+            pltpu.VMEM((n_ep, n_tp, capacity, width), bf16),
+            pltpu.VMEM((n_ep, 2, capacity, width), bf16),
+            pltpu.VMEM((n_ep, capacity, width), bf16),
+            pltpu.VMEM((n_ep, capacity, width), bf16),
+            pltpu.VMEM((n_ep, capacity, width), bf16),
+            pltpu.VMEM((n_ep * n_tp * own_rows, key_up.shape[1] + rope_room), bf16),
+            pltpu.VMEM((n_tp, own_rows, value_up.shape[1]), bf16),
+            pltpu.VMEM((n_tp, own_rows, value_up.shape[1]), bf16),
+            pltpu.VMEM(out_proj.shape, bf16),
+            pltpu.VMEM(w_gate.shape[1:], bf16),
+            pltpu.VMEM(w_up.shape[1:], bf16),
+            pltpu.VMEM(w_down.shape[1:], bf16),
+            pltpu.SemaphoreType.DMA((6,)),
+            pltpu.SemaphoreType.DMA((12, n_ep)),
+            pltpu.SemaphoreType.DMA((12, n_ep)),
+            pltpu.SemaphoreType.DMA((3,)),
+            pltpu.SemaphoreType.DMA((3,)),
+        ],
+        compiler_params=pltpu.CompilerParams(
+            collective_id=0, has_side_effects=True, vmem_limit_bytes=56 * 1024 * 1024
+        ),
+        name="both_halves",
+    )(
+        outgoing,
+        lat_own,
+        query_big,
+        key_up,
+        value_up,
+        out_proj,
+        w_gate[0],
+        w_up[0],
+        w_down[0],
+    )
+    flat = returned.reshape(n_ep * capacity, width)
+    picked = flat[target].reshape(row_count, top_count, width).astype(jnp.float32)
+    shares = group_prob[:, None] * expert_prob / jnp.sum(expert_prob, axis=1, keepdims=True)
+    moe_out = jnp.sum(shares[:, :, None] * picked, axis=1).astype(bf16)
+    return (mixed, moe_out)
+
+
+def fits_kernel(mesh, *arrays):
+    n_ep, n_tp = mesh.shape["ep"], mesh.shape["tp"]
+    tokens, routes, latent = arrays[7], arrays[9], arrays[1]
+    capacity = 2 * routes.shape[1] * tokens.shape[0] // (n_ep * n_tp) // n_ep
+    own_rows = latent.shape[0] // (n_ep * n_tp)
+    packed = latent.shape[0] <= 2048
+    return n_tp == 4 and capacity % 16 == 0 and own_rows % 16 == 0 and packed
+
+
+def mapped(mesh, chosen):
     return jax.shard_map(
-        body,
+        chosen,
         mesh=mesh,
         in_specs=(
             P("ep", "tp"),
@@ -227,3 +671,11 @@
         out_specs=(P(("ep", "tp"), None), P(("ep", "tp"), None)),
         check_vma=False,
     )
+
+
+def solution(mesh):
+    def whole(*arrays):
+        chosen = fused_body if fits_kernel(mesh, *arrays) else body
+        return mapped(mesh, chosen)(*arrays)
+
+    return whole

time: 225 us -> 107 us (0.48)
  Pallas kernels: 0 us -> 88.5 us
  blocking collectives: 81.1 us -> 0 us
  waiting for transfers between devices: 79.3 us -> 0 us
  matrix products: 25.4 us -> 2.2 us
  between operations: 14 us -> 0.88 us
  starting transfers between devices: 5.53 us -> 0 us
    pallas_call x0 -> x1, Pallas kernels: none -> 88.5 us  [fused_body(): pl.pallas_call(functools.partial(both_halves, heads, ROPE_DIM), out_shape...]
    all_gather x1 -> x0, blocking collectives: 41.5 us -> none  [mixer_half(): lax.all_gather(rotated_key, ('ep', 'tp'), axis=0, tiled=True)]
    all_to_all x2 -> x0, blocking collectives: 39.6 us -> none  [the longest x1 33 us: expert_half(): lax.all_to_all(outgoing, 'ep', split_axis=0, concat_axis=0, tiled=True)]
    all_gather x2 -> x0, waiting for transfers between devices: 33.7 us -> none  [the longest x1 32.6 us: expert_half(): shard_rows = lax.all_gather(flat_rows, 'tp', axis=0, tiled=True)]
    reduce_scatter x1 -> x0, waiting for transfers between devices: 23.9 us -> none  [expert_half(): lax.psum_scatter(lower(jnp.int32(0), sources * slots * lax.axis_size('tp'...]
    dot_general x8 -> x1, matrix products: 25.4 us -> 2.2 us  [fused_body(): jnp.dot(dispatch_table, normed, preferred_element_type=jnp.float32)]
    all_to_all x1 -> x0, waiting for transfers between devices: 21.7 us -> none  [expert_half(): lax.all_to_all(result, 'ep', split_axis=0, concat_axis=0, tiled=True)]
    all_to_all x1 -> x0, starting transfers between devices: 5.41 us -> none  [expert_half(): lax.all_to_all(result, 'ep', split_axis=0, concat_axis=0, tiled=True)]
  transfers between devices with their start and end apart: 4 -> 0, of which waited for: 4 -> 0; matrix products, arithmetic and copies ran while one was open for 14% -> 0% of each run, Pallas kernels for 0% -> 0%
where the time goes in v1:
time: 107 us
  Pallas kernels  88.5 us (83%)
  other arithmetic  8.19 us (8%)
  local copies, waits for them, and re-layouts  6.97 us (7%)
  matrix products  2.2 us (2%)
    pallas_call x1, Pallas kernels, fused_body(): pl.pallas_call(functools.partial(both_halves, heads, ROPE_DIM), out_shape...  88.5 us
    gather x1, local copies, waits for them, and re-layouts, fused_body(): flat[target].reshape(row_count, top_count, width).astype(jnp.float32)  2.8 us
    unnamed x11, local copies, waits for them, and re-layouts  2.46 us
    reduce_sum x1, other arithmetic, fused_body(): moe_out = jnp.sum(shares[:, :, None] * picked, axis=1).astype(bf16)  2.23 us
    dot_general x1, matrix products, fused_body(): jnp.dot(dispatch_table, normed, preferred_element_type=jnp.float32)  2.2 us

profile of v1, /device:TPU:0, one launch (start us, length us, event | category | flops | bytes accessed | tf_op | source)
XLA Modules:
  0.0 106.7 jit_solution(12019900092885629430)
XLA Ops:
  0.7 0.1 multiply_cosine_fusion.1
  0.8 1.0 copy.44
  1.9 0.1 copy.46
  2.1 0.1 copy.45
  2.4 0.8 fusion.4.query_big
  3.2 0.7 convert_element_type.60
  3.9 0.1 fusion.18
  4.2 0.9 fusion.9
  5.0 0.8 fusion.11
  5.9 0.6 pad_maximum_fusion.lat_own
  6.5 0.8 copy.40
  7.3 0.1 eq.36
  7.5 0.2 reduce_window_sum.11
  7.7 0.2 select_reduce_fusion
  7.9 0.1 reduce_sum.50
  8.1 0.1 fusion.8
  8.2 1.1 %fusion.1 = f32[64]{0:T(128)S(1)} fusion(bf16[64,2048]{1,0:T(8,128)(2,1)} %param.22), kind=kLoop, calls=%fused_computation.7 | loop fusion | flops 393152 | bytes 262400 | tf_op jit(solution)/shard_map/reduce_sum | solution.py:23
  9.3 2.2 %convolution_convert_fusion = bf16[256,2048]{1,0:T(8,128)(2,1)} fusion(pred[256,64]{0,1:T(8,128)(4,1)S(1)} %fusion.8, bf16[64,2048]{1,0:T(8,128)(2,1)S(1)} %copy-done, f32[2048]{0:T(1024)} %param.23, f32[64]{0:T(128)S(1)} %add_rsqrt_fusion.1), kind=kOutput, calls=%fused_computation.1 | convolution fusion | flops 68157440 | bytes 1335552 | tf_op jit(solution)/shard_map/dot_general | solution.py:581
  11.5 88.5 %both_halves.1 = (bf16[32,2048]{1,0:T(8,128)(2,1)}, bf16[8,32,2048]{2,1,0:T(8,128)(2,1)}) custom-call(bf16[8,32,2048]{2,1,0:T(8,128)(2,1)} %bitcast.17, bf16[32,640]{1,0:T(8,128)(2,1)} %pad_maximum_fusion.lat_own, bf16[4,128,384]{2,1,0:T(8,128)(2,1)} %fusion.4.query_big, bf16[512,256]{1,0:T(8,128)(2,1)} %key_up.1, bf16[512,256]{1,0:T(8,128)(2,1)} %value_up.1, ...), custom_call_target="tpu_custom_call" | custom-call | tf_op jit(solution)/shard_map/both_halves/pallas_call | solution.py:590
  100.1 0.1 mul.193
  100.2 2.8 %gather_fusion = bf16[128,2048]{1,0:T(8,128)(2,1)S(1)} fusion(bf16[256,2048]{1,0:T(8,128)(2,1)} %bitcast.16, s32[1024]{0:T(1024)S(1)} %pad_clamp_fusion), kind=kCustom, calls=%fused_computation | custom fusion | bytes 1049088 | tf_op jit(solution)/shard_map/gather | solution.py:635
  103.0 0.7 reshape.168
  103.8 2.2 %multiply_reduce_fusion = bf16[64,2048]{1,0:T(8,128)(2,1)} fusion(f32[64,2,2048]{2,1,0:T(2,128)S(1)} %reshape.168, f32[64,2]{1,0:T(8,128)S(1)} %copy.47), kind=kLoop, calls=%fused_computation.2 | loop fusion | flops 393216 | bytes 1311232 | tf_op jit(solution)/shard_map/reduce_sum | solution.py:637
  106.1 0.7 copy.49
  (31 shorter events, 0.7 us)
Async XLA Ops:
  0.6 8.7 %copy-start = (bf16[64,2048]{1,0:T(8,128)(2,1)S(1)}, bf16[64,2048]{1,0:T(8,128)(2,1)}, u32[]{:S(2)}) copy-start(bf16[64,2048]{1,0:T(8,128)(2,1)} %param.22) | copy-start | bytes 786436
  100.0 3.7 %copy-start.2 = (f32[64,2]{0,1:T(2,128)S(1)}, f32[64,2]{0,1:T(2,128)}, u32[]{:S(2)}) copy-start(f32[64,2]{0,1:T(2,128)} %param.26) | copy-start | bytes 1540
  100.0 3.7 %copy-start.3 = (f32[64]{0:T(128)S(1)}, f32[64]{0:T(128)}, u32[]{:S(2)}) copy-start(f32[64]{0:T(128)} %param.25) | copy-start | bytes 772
  100.0 6.0 %copy-start.1 = (bf16[32,2048]{1,0:T(8,128)(2,1)S(1)}, bf16[32,2048]{1,0:T(8,128)(2,1)}, u32[]{:S(2)}) copy-start(bf16[32,2048]{1,0:T(8,128)(2,1)} %get-tuple-element.16) | copy-start | bytes 393220

commit v2 on v1

--- a/solution.py
+++ b/solution.py
@@ -218,8 +218,13 @@
     gate_hbm,
     up_hbm,
     down_hbm,
+    slots,
+    shares,
     mixed,
+    moe_out,
     returned,
+    relay_in,
+    relay_back,
     arrived,
     lat_all,
     partial,
@@ -241,9 +246,13 @@
     head_recv,
 ):
     experts, capacity, width = outgoing.shape
-    n_tp = lat_all.shape[1]
+    n_tp = lat_all.shape[2]
+    depth_z = experts // 2
+    middle = depth_z + 1 if depth_z == 4 else experts
     me = lax.axis_index("ep")
     tp = lax.axis_index("tp")
+    me_z = me // 2
+    me_y = me % 2
     mate = tp + 1 - 2 * (tp % 2)
     far = (tp + 2) % n_tp
     cross = (mate + 2) % n_tp
@@ -254,7 +263,7 @@
         pltpu.make_async_copy(down_hbm, down, load_sem.at[2]),
         pltpu.make_async_copy(out_proj_hbm, out_proj, load_sem.at[3]),
         pltpu.make_async_copy(outgoing.at[me], arrived.at[me, tp], load_sem.at[4]),
-        pltpu.make_async_copy(lat_own, lat_all.at[me, tp], load_sem.at[5]),
+        pltpu.make_async_copy(lat_own, lat_all.at[me_z, me_y, tp], load_sem.at[5]),
     ]
     for load in loads:
         load.start()
@@ -269,6 +278,18 @@
             device_id_type=pl.DeviceIdType.MESH,
         )
 
+    def ahead(step):
+        return (me_z + step // 2) % depth_z * 2 + (me_y + step) % 2
+
+    def behind(step):
+        return (me_z + depth_z - step // 2) % depth_z * 2 + (me_y + step) % 2
+
+    below = (me_z + depth_z - 1) % depth_z * 2
+    above = (me_z + 1) % depth_z * 2
+    relay_peer = below + 1 - me_y
+    relay_end = below + me_y
+    relay_from = above + 1 - me_y
+
     barrier = pltpu.get_barrier_semaphore()
 
     def greet(step, carry):
@@ -288,45 +309,75 @@
     pl.semaphore_wait(barrier, experts + 2)
 
     def ep_rows(step, slot):
-        target = (me + step) % experts
+        target = ahead(step)
         return remote(outgoing.at[target], arrived.at[slot, tp], 0, step, {"ep": target})
 
-    def ep_lat(step, slot):
-        target = (me + step) % experts
-        return remote(lat_own, lat_all.at[slot, tp], 1, step, {"ep": target})
+    def rows_out():
+        return remote(
+            outgoing.at[ahead(middle)], relay_in, 0, middle, {"ep": relay_peer}
+        )
+
+    def rows_on(slot):
+        return remote(relay_in, arrived.at[slot, tp], 12, middle, {"ep": relay_end})
+
+    def back_out():
+        return remote(
+            result.at[behind(middle)], relay_back, 11, middle, {"ep": relay_peer}
+        )
+
+    def back_on(slot):
+        return remote(relay_back, returned.at[slot], 13, middle, {"ep": relay_end})
+
+    def lat_x(block):
+        return remote(lat_own, lat_all.at[me_z, me_y, block], 5, 0, {"tp": far})
+
+    def lat_z(shift, part, origin):
+        block = (tp + 2 * part) % n_tp
+        target = (me_z + shift) % depth_z * 2 + me_y
+        return remote(
+            lat_all.at[me_z, me_y, block],
+            lat_all.at[origin, me_y, block],
+            1,
+            shift * 2 + part,
+            {"ep": target},
+        )
+
+    def lat_y(part, side):
+        place = lat_all.at[:, side, (tp + 2 * part) % n_tp]
+        return remote(place, place, 3, part, {"ep": me_z * 2 + 1 - me_y})
+
+    def lat_mate(part, first):
+        place = lat_all.at[:, :, (first + 2 * part) % n_tp]
+        return remote(place, place, 7, part, {"tp": mate})
 
     def hop_rows(kind, step, block, peer):
-        source = (me + experts - step) % experts
+        source = behind(step)
         place = arrived.at[source, block]
         return remote(place, place, kind, step, {"tp": peer})
 
-    def hop_lat(kind, step, block, peer):
-        source = (me + experts - step) % experts
-        place = lat_all.at[source, block]
-        return remote(place, place, kind, step, {"tp": peer})
-
     def to_mate(kind, step, block, part):
-        source = (me + experts - step) % experts
+        source = behind(step)
         return remote(
             partial.at[source, block], from_pair.at[source, part], kind, step, {"tp": mate}
         )
 
     def to_far(step):
-        source = (me + experts - step) % experts
+        source = behind(step)
         return remote(pair_sum.at[source], from_far.at[source], 10, step, {"tp": far})
 
     def back(step, slot):
-        source = (me + experts - step) % experts
+        source = behind(step)
         return remote(result.at[source], returned.at[slot], 11, step, {"ep": source})
 
-    def send_all(step, carry):
-        ep_lat(step, me).start()
-        return carry
-
-    lax.fori_loop(1, experts, send_all, 0)
+    lat_x(tp).start()
+    if middle < experts:
+        rows_out().start()
 
     def send_rows(step, carry):
-        ep_rows(step, me).start()
+        @pl.when(step != middle)
+        def _():
+            ep_rows(step, me).start()
+
         return carry
 
     lax.fori_loop(1, experts, send_rows, 0)
@@ -334,29 +385,28 @@
         load.wait()
 
     def forward(step):
-        source = (me + experts - step) % experts
-
-        @pl.when(step > 0)
-        def _():
-            ep_lat(step, source).wait_recv()
+        source = behind(step)
+
+        @pl.when((step > 0) & (step != middle))
+        def _():
             ep_rows(step, source).wait_recv()
 
-        hop_lat(5, step, tp, far).start()
+        if middle < experts:
+
+            @pl.when(step == middle)
+            def _():
+                rows_on(source).wait_recv()
+
         hop_rows(4, step, tp, far).start()
-        hop_lat(3, step, tp, mate).start()
         hop_rows(2, step, tp, mate).start()
 
     def relay(step):
-        hop_lat(5, step, far, far).wait_recv()
         hop_rows(4, step, far, far).wait_recv()
-        hop_lat(7, step, far, mate).start()
         hop_rows(6, step, far, mate).start()
 
     def compute(step):
-        source = (me + experts - step) % experts
-        hop_lat(3, step, mate, mate).wait_recv()
+        source = behind(step)
         hop_rows(2, step, mate, mate).wait_recv()
-        hop_lat(7, step, cross, mate).wait_recv()
         hop_rows(6, step, cross, mate).wait_recv()
 
         @pl.when(step == 0)
@@ -374,7 +424,7 @@
         to_mate(8, step, mate, 0).start()
 
     def reduce_pair(step):
-        source = (me + experts - step) % experts
+        source = behind(step)
         to_mate(9, step, cross, 1).wait_recv()
         pair_sum[source] = (
             partial[source, far].astype(jnp.float32) + from_pair[source, 1].astype(jnp.float32)
@@ -382,7 +432,7 @@
         to_far(step).start()
 
     def reduce_far(step):
-        source = (me + experts - step) % experts
+        source = behind(step)
         to_mate(8, step, mate, 0).wait_recv()
         to_far(step).wait_recv()
         result[source] = (
@@ -391,9 +441,15 @@
             + from_far[source].astype(jnp.float32)
         ).astype(jnp.bfloat16)
 
-        @pl.when(step > 0)
+        @pl.when((step > 0) & (step != middle))
         def _():
             back(step, me).start()
+
+        if middle < experts:
+
+            @pl.when(step == middle)
+            def _():
+                back_out().start()
 
         @pl.when(step == 0)
         def _():
@@ -470,10 +526,52 @@
         def _():
             reduce_far(turn - 4)
 
+        @pl.when(turn == 1)
+        def _():
+            lat_x(far).wait_recv()
+
+            def spread(shift, inner):
+                lat_z(shift, 0, me_z).start()
+                lat_z(shift, 1, me_z).start()
+                return inner
+
+            lax.fori_loop(1, depth_z, spread, 0)
+
+        @pl.when(turn == experts - 1)
+        def _():
+            def collect(shift, inner):
+                origin = (me_z + depth_z - shift) % depth_z
+                lat_z(shift, 0, origin).wait_recv()
+                lat_z(shift, 1, origin).wait_recv()
+                return inner
+
+            lax.fori_loop(1, depth_z, collect, 0)
+            lat_y(0, me_y).start()
+            lat_y(1, me_y).start()
+
+        @pl.when(turn == experts + 1)
+        def _():
+            lat_y(0, 1 - me_y).wait_recv()
+            lat_y(1, 1 - me_y).wait_recv()
+            lat_mate(0, tp).start()
+            lat_mate(1, tp).start()
+
+        if middle < experts:
+
+            @pl.when(turn == 2)
+            def _():
+                rows_out().wait_recv()
+                rows_on(relay_from).start()
+
         return carry
 
     lax.fori_loop(0, experts + 4, stage, 0)
 
+    if middle < experts:
+        back_out().wait_recv()
+        back_on(relay_from).start()
+    lat_mate(0, mate).wait_recv()
+    lat_mate(1, mate).wait_recv()
     attend()
     peers = (mate, far, cross)
     for number, peer in enumerate(peers):
@@ -493,20 +591,59 @@
     mixed[...] = total.astype(mixed.dtype)
 
     def finish(step, carry):
-        ep_lat(step, me).wait_send()
-        ep_rows(step, me).wait_send()
-        back(step, me).wait_send()
-        back(step, (me + step) % experts).wait_recv()
+        @pl.when(step != middle)
+        def _():
+            back(step, ahead(step)).wait_recv()
+
+        if middle < experts:
+
+            @pl.when(step == middle)
+            def _():
+                back_on(ahead(middle)).wait_recv()
+
         return carry
 
     lax.fori_loop(1, experts, finish, 0)
 
+    answers = returned[...].reshape(experts * capacity, width)
+    row = lax.broadcasted_iota(jnp.int32, (slots.shape[0], experts * capacity), 1)
+    chosen = jnp.zeros(moe_out.shape, jnp.float32)
+    for pick in range(slots.shape[1]):
+        table = jnp.where(row == slots[:, pick : pick + 1], 1.0, 0.0).astype(jnp.bfloat16)
+        chosen = chosen + shares[:, pick : pick + 1] * jnp.dot(
+            table, answers, preferred_element_type=jnp.float32
+        )
+    moe_out[...] = chosen.astype(moe_out.dtype)
+
+    def finish_ep(step, carry):
+        @pl.when(step != middle)
+        def _():
+            ep_rows(step, me).wait_send()
+            back(step, me).wait_send()
+
+        return carry
+
+    lax.fori_loop(1, experts, finish_ep, 0)
+    if middle < experts:
+        rows_out().wait_send()
+        rows_on(relay_from).wait_send()
+        back_out().wait_send()
+        back_on(relay_from).wait_send()
+    lat_x(tp).wait_send()
+
+    def finish_lat(shift, carry):
+        lat_z(shift, 0, me_z).wait_send()
+        lat_z(shift, 1, me_z).wait_send()
+        return carry
+
+    lax.fori_loop(1, depth_z, finish_lat, 0)
+    for part in range(2):
+        lat_y(part, me_y).wait_send()
+        lat_mate(part, tp).wait_send()
+
     def finish_tp(step, carry):
-        hop_lat(5, step, tp, far).wait_send()
         hop_rows(4, step, tp, far).wait_send()
-        hop_lat(3, step, tp, mate).wait_send()
         hop_rows(2, step, tp, mate).wait_send()
-        hop_lat(7, step, far, mate).wait_send()
         hop_rows(6, step, far, mate).wait_send()
         to_mate(9, step, cross, 1).wait_send()
         to_mate(8, step, mate, 0).wait_send()
@@ -583,21 +720,25 @@
     )
     outgoing = outgoing.reshape(n_ep, capacity, width)
 
+    shares = group_prob[:, None] * expert_prob / jnp.sum(expert_prob, axis=1, keepdims=True)
     bf16 = jnp.bfloat16
     lat_width = latent_width + rope_room
     vmem = pl.BlockSpec(memory_space=pltpu.VMEM)
     anywhere = pl.BlockSpec(memory_space=pl.ANY)
-    mixed, returned = pl.pallas_call(
+    mixed, moe_out = pl.pallas_call(
         functools.partial(both_halves, heads, ROPE_DIM),
         out_shape=(
             jax.ShapeDtypeStruct((own_rows, out_proj.shape[1]), bf16),
-            jax.ShapeDtypeStruct((n_ep, capacity, width), bf16),
+            jax.ShapeDtypeStruct((row_count, width), bf16),
         ),
-        in_specs=[vmem] * 5 + [anywhere] * 4,
+        in_specs=[vmem] * 5 + [anywhere] * 4 + [vmem] * 2,
         out_specs=(vmem, vmem),
         scratch_shapes=[
+            pltpu.VMEM((n_ep, capacity, width), bf16),
+            pltpu.VMEM((capacity, width), bf16),
+            pltpu.VMEM((capacity, width), bf16),
             pltpu.VMEM((n_ep, n_tp, capacity, width), bf16),
-            pltpu.VMEM((n_ep, n_tp, own_rows, lat_width), bf16),
+            pltpu.VMEM((n_ep // 2, 2, n_tp, own_rows, lat_width), bf16),
             pltpu.VMEM((n_ep, n_tp, capacity, width), bf16),
             pltpu.VMEM((n_ep, 2, capacity, width), bf16),
             pltpu.VMEM((n_ep, capacity, width), bf16),
@@ -611,8 +752,8 @@
             pltpu.VMEM(w_up.shape[1:], bf16),
             pltpu.VMEM(w_down.shape[1:], bf16),
             pltpu.SemaphoreType.DMA((6,)),
-            pltpu.SemaphoreType.DMA((12, n_ep)),
-            pltpu.SemaphoreType.DMA((12, n_ep)),
+            pltpu.SemaphoreType.DMA((14, n_ep)),
+            pltpu.SemaphoreType.DMA((14, n_ep)),
             pltpu.SemaphoreType.DMA((3,)),
             pltpu.SemaphoreType.DMA((3,)),
         ],
@@ -630,11 +771,9 @@
         w_gate[0],
         w_up[0],
         w_down[0],
-    )
-    flat = returned.reshape(n_ep * capacity, width)
-    picked = flat[target].reshape(row_count, top_count, width).astype(jnp.float32)
-    shares = group_prob[:, None] * expert_prob / jnp.sum(expert_prob, axis=1, keepdims=True)
-    moe_out = jnp.sum(shares[:, :, None] * picked, axis=1).astype(bf16)
+        target.reshape(row_count, top_count),
+        shares,
+    )
     return (mixed, moe_out)
 
 
@@ -644,7 +783,7 @@
     capacity = 2 * routes.shape[1] * tokens.shape[0] // (n_ep * n_tp) // n_ep
     own_rows = latent.shape[0] // (n_ep * n_tp)
     packed = latent.shape[0] <= 2048
-    return n_tp == 4 and capacity % 16 == 0 and own_rows % 16 == 0 and packed
+    return n_tp == 4 and n_ep >= 8 and n_ep % 2 == 0 and capacity % 16 == 0 and own_rows % 16 == 0 and packed
 
 
 def mapped(mesh, chosen):

time: 107 us -> 94 us (0.88)
  Pallas kernels: 88.5 us -> 77.2 us
    pallas_call x1, Pallas kernels: 88.5 us -> 77.2 us  [fused_body(): pl.pallas_call(functools.partial(both_halves, heads, ROPE_DIM), out_shape...]
    gather x1 -> x0, local copies, waits for them, and re-layouts: 2.8 us -> none  [fused_body(): flat[target].reshape(row_count, top_count, width).astype(jnp.float32)]
    unnamed x11 -> x10, local copies, waits for them, and re-layouts: 2.46 us -> 5.03 us
    reduce_sum x1 -> x0, other arithmetic: 2.23 us -> none  [fused_body(): moe_out = jnp.sum(shares[:, :, None] * picked, axis=1).astype(bf16)]
where the time goes in v2:
time: 94 us; the launch traced here: 93.6 us
  Pallas kernels  77.2 us (82%)
  other arithmetic  8 us (9%)
  local copies, waits for them, and re-layouts  6.06 us (6%)
  matrix products  1.49 us (2%)
    pallas_call x1, Pallas kernels, fused_body(): pl.pallas_call(functools.partial(both_halves, heads, ROPE_DIM), out_shape...  77.2 us
    unnamed x10, local copies, waits for them, and re-layouts  5.03 us
    reduce_sum x2, other arithmetic, rms_scale(): jnp.mean(widened * widened, axis=-1, keepdims=True) + epsilon  2.02 us

profile of v2, /device:TPU:0, one launch (start us, length us, event | category | flops | bytes accessed | tf_op | source)
XLA Modules:
  0.0 93.6 jit_solution(4871365175810143847)
XLA Ops:
  0.7 0.9 fusion.9
  1.6 1.1 %fusion.1 = f32[64]{0:T(128)S(1)} fusion(bf16[64,2048]{1,0:T(8,128)(2,1)} %param.22), kind=kLoop, calls=%fused_computation.5 | loop fusion | flops 393152 | bytes 262400 | tf_op jit(solution)/shard_map/reduce_sum | solution.py:23
  2.8 0.7 broadcast_multiply_fusion.1
  3.6 0.7 fusion.24
  4.3 0.1 multiply_cosine_fusion.1
  4.4 0.7 convert_element_type.51
  5.1 0.1 fusion.18
  5.4 0.8 fusion.11
  6.3 0.6 pad_maximum_fusion.lat_own
  7.0 0.7 broadcast_divide_fusion.shares
  7.7 0.8 copy.48
  8.5 0.1 eq.36
  8.7 0.2 reduce_window_sum.11
  8.9 0.2 select_reduce_fusion
  9.0 0.1 reduce_sum.39
  9.3 0.1 fusion.8
  9.4 1.0 %copy.52 = bf16[128,384]{0,1:T(8,128)(2,1)S(1)} copy(bf16[128,384]{1,0:T(8,128)(2,1)} %param.15) | data formatting | bytes 196608 | tf_op args[0]
  10.5 0.1 copy.54
  10.7 0.1 copy.53
  10.8 0.8 fusion.4.query_big
  11.6 1.5 %convolution_convert_fusion = bf16[256,2048]{1,0:T(8,128)(2,1)} fusion(pred[256,64]{0,1:T(8,128)(4,1)S(1)} %fusion.8, bf16[64,2048]{1,0:T(8,128)(2,1)S(1)} %copy-done, f32[2048]{0:T(1024)S(1)} %copy-done.2, f32[64]{0:T(128)S(1)} %add_rsqrt_fusion.1), kind=kOutput, calls=%fused_computation | convolution fusion | flops 68157440 | bytes 1335552 | tf_op jit(solution)/shard_map/dot_general | solution.py:718
  13.1 77.2 %both_halves.1 = (bf16[32,2048]{1,0:T(8,128)(2,1)}, bf16[64,2048]{1,0:T(8,128)(2,1)}) custom-call(bf16[8,32,2048]{2,1,0:T(8,128)(2,1)} %bitcast.9, bf16[32,640]{1,0:T(8,128)(2,1)} %pad_maximum_fusion.lat_own, bf16[4,128,384]{2,1,0:T(8,128)(2,1)} %fusion.4.query_big, bf16[512,256]{1,0:T(8,128)(2,1)} %key_up.1, bf16[512,256]{1,0:T(8,128)(2,1)} %value_up.1, ...), custom_call_target="tpu_custom_call" | custom-call | tf_op jit(solution)/shard_map/both_halves/pallas_call | solution.py:728
  90.3 1.6 %copy.59 = bf16[32,2048]{1,0:T(8,128)(2,1)} copy(bf16[32,2048]{1,0:T(8,128)(2,1)} %get-tuple-element.12) | data formatting | bytes 262144
  91.9 1.7 %copy.60 = bf16[64,2048]{1,0:T(8,128)(2,1)} copy(bf16[64,2048]{1,0:T(8,128)(2,1)} %get-tuple-element.13) | data formatting | bytes 524288
  (26 shorter events, 0.8 us)
Async XLA Ops:
  0.6 11.0 %copy-start = (bf16[64,2048]{1,0:T(8,128)(2,1)S(1)}, bf16[64,2048]{1,0:T(8,128)(2,1)}, u32[]{:S(2)}) copy-start(bf16[64,2048]{1,0:T(8,128)(2,1)} %param.22) | copy-start | bytes 786436
  0.6 11.0 %copy-start.2 = (f32[2048]{0:T(1024)S(1)}, f32[2048]{0:T(1024)}, u32[]{:S(2)}) copy-start(f32[2048]{0:T(1024)} %param.23) | copy-start | bytes 24580
  9.2 3.9 %copy-start.1 = (s32[64,2]{1,0:T(8,128)}, s32[64,2]{1,0:T(8,128)S(1)}, u32[]{:S(2)}) copy-start(s32[64,2]{1,0:T(8,128)S(1)} %add.63.slots) | copy-start | bytes 1540

commit v3 on v2

--- a/solution.py
+++ b/solution.py
@@ -506,25 +506,25 @@
         )
 
     def stage(turn, carry):
+        @pl.when(turn >= 4)
+        def _():
+            reduce_far(turn - 4)
+
+        @pl.when((turn >= 3) & (turn < experts + 3))
+        def _():
+            reduce_pair(turn - 3)
+
+        @pl.when((turn >= 2) & (turn < experts + 2))
+        def _():
+            compute(turn - 2)
+
+        @pl.when((turn >= 1) & (turn < experts + 1))
+        def _():
+            relay(turn - 1)
+
         @pl.when(turn < experts)
         def _():
             forward(turn)
-
-        @pl.when((turn >= 1) & (turn < experts + 1))
-        def _():
-            relay(turn - 1)
-
-        @pl.when((turn >= 2) & (turn < experts + 2))
-        def _():
-            compute(turn - 2)
-
-        @pl.when((turn >= 3) & (turn < experts + 3))
-        def _():
-            reduce_pair(turn - 3)
-
-        @pl.when(turn >= 4)
-        def _():
-            reduce_far(turn - 4)
 
         @pl.when(turn == 1)
         def _():
@@ -563,13 +563,17 @@
                 rows_out().wait_recv()
                 rows_on(relay_from).start()
 
+        if middle < experts:
+
+            @pl.when(turn == experts + 2)
+            def _():
+                back_out().wait_recv()
+                back_on(relay_from).start()
+
         return carry
 
     lax.fori_loop(0, experts + 4, stage, 0)
 
-    if middle < experts:
-        back_out().wait_recv()
-        back_on(relay_from).start()
     lat_mate(0, mate).wait_recv()
     lat_mate(1, mate).wait_recv()
     attend()

time: 94 us -> 91.7 us (0.976)
  Pallas kernels: 77.2 us -> 74.9 us
    pallas_call x1, Pallas kernels: 77.2 us -> 74.9 us  [fused_body(): pl.pallas_call(functools.partial(both_halves, heads, ROPE_DIM), out_shape...]
where the time goes in v3:
time: 91.7 us; the launch traced here: 91.2 us
  Pallas kernels  74.9 us (82%)
  other arithmetic  8 us (9%)
  local copies, waits for them, and re-layouts  6.06 us (7%)
  matrix products  1.49 us (2%)
    pallas_call x1, Pallas kernels, fused_body(): pl.pallas_call(functools.partial(both_halves, heads, ROPE_DIM), out_shape...  74.9 us
    unnamed x10, local copies, waits for them, and re-layouts  5.03 us
    reduce_sum x2, other arithmetic, rms_scale(): jnp.mean(widened * widened, axis=-1, keepdims=True) + epsilon  2.02 us

profile of v3, /device:TPU:0, one launch (start us, length us, event | category | flops | bytes accessed | tf_op | source)
XLA Modules:
  0.0 91.2 jit_solution(6871711346000919405)
XLA Ops:
  0.7 0.9 fusion.9
  1.6 1.1 %fusion.1 = f32[64]{0:T(128)S(1)} fusion(bf16[64,2048]{1,0:T(8,128)(2,1)} %param.22), kind=kLoop, calls=%fused_computation.5 | loop fusion | flops 393152 | bytes 262400 | tf_op jit(solution)/shard_map/reduce_sum | solution.py:23
  2.8 0.7 broadcast_multiply_fusion.1
  3.6 0.7 fusion.24
  4.3 0.1 multiply_cosine_fusion.1
  4.4 0.7 convert_element_type.51
  5.1 0.1 fusion.18
  5.4 0.8 fusion.11
  6.3 0.6 pad_maximum_fusion.lat_own
  7.0 0.7 broadcast_divide_fusion.shares
  7.7 0.8 copy.48
  8.5 0.1 eq.36
  8.7 0.2 reduce_window_sum.11
  8.9 0.2 select_reduce_fusion
  9.0 0.1 reduce_sum.39
  9.3 0.1 fusion.8
  9.4 1.0 %copy.52 = bf16[128,384]{0,1:T(8,128)(2,1)S(1)} copy(bf16[128,384]{1,0:T(8,128)(2,1)} %param.15) | data formatting | bytes 196608 | tf_op args[0]
  10.5 0.1 copy.54
  10.7 0.1 copy.53
  10.8 0.8 fusion.4.query_big
  11.6 1.5 %convolution_convert_fusion = bf16[256,2048]{1,0:T(8,128)(2,1)} fusion(pred[256,64]{0,1:T(8,128)(4,1)S(1)} %fusion.8, bf16[64,2048]{1,0:T(8,128)(2,1)S(1)} %copy-done, f32[2048]{0:T(1024)S(1)} %copy-done.2, f32[64]{0:T(128)S(1)} %add_rsqrt_fusion.1), kind=kOutput, calls=%fused_computation | convolution fusion | flops 68157440 | bytes 1335552 | tf_op jit(solution)/shard_map/dot_general | solution.py:722
  13.1 74.9 %both_halves.1 = (bf16[32,2048]{1,0:T(8,128)(2,1)}, bf16[64,2048]{1,0:T(8,128)(2,1)}) custom-call(bf16[8,32,2048]{2,1,0:T(8,128)(2,1)} %bitcast.9, bf16[32,640]{1,0:T(8,128)(2,1)} %pad_maximum_fusion.lat_own, bf16[4,128,384]{2,1,0:T(8,128)(2,1)} %fusion.4.query_big, bf16[512,256]{1,0:T(8,128)(2,1)} %key_up.1, bf16[512,256]{1,0:T(8,128)(2,1)} %value_up.1, ...), custom_call_target="tpu_custom_call" | custom-call | tf_op jit(solution)/shard_map/both_halves/pallas_call | solution.py:732
  88.0 1.6 %copy.59 = bf16[32,2048]{1,0:T(8,128)(2,1)} copy(bf16[32,2048]{1,0:T(8,128)(2,1)} %get-tuple-element.12) | data formatting | bytes 262144
  89.6 1.7 %copy.60 = bf16[64,2048]{1,0:T(8,128)(2,1)} copy(bf16[64,2048]{1,0:T(8,128)(2,1)} %get-tuple-element.13) | data formatting | bytes 524288
  (26 shorter events, 0.8 us)
Async XLA Ops:
  0.6 11.0 %copy-start = (bf16[64,2048]{1,0:T(8,128)(2,1)S(1)}, bf16[64,2048]{1,0:T(8,128)(2,1)}, u32[]{:S(2)}) copy-start(bf16[64,2048]{1,0:T(8,128)(2,1)} %param.22) | copy-start | bytes 786436
  0.6 11.0 %copy-start.2 = (f32[2048]{0:T(1024)S(1)}, f32[2048]{0:T(1024)}, u32[]{:S(2)}) copy-start(f32[2048]{0:T(1024)} %param.23) | copy-start | bytes 24580
  9.2 3.9 %copy-start.1 = (s32[64,2]{1,0:T(8,128)}, s32[64,2]{1,0:T(8,128)S(1)}, u32[]{:S(2)}) copy-start(s32[64,2]{1,0:T(8,128)S(1)} %add.63.slots) | copy-start | bytes 1540
